TPU v7x, 32 devices: a whole 2x2x4 slice. The times are simulated.
32 devices in a mesh: sp: 8 (over z, y), fs: 2 (over x), tp: 2 (over core).
Axes of the slice: x: 2, y: 2, z: 4, core: 2. Of those that a mesh axis runs over, the one named last changes fastest.
Arguments:
- tokens: bfloat16 [8192, 2048], P(('fs', 'sp', 'tp')), parts along dimension 0, may hold values from -60 to 60
- norm_gain: float32 [2048], replicated, may hold values from 0.1 to 1.9
- pool_in: bfloat16 [2048, 512], P('sp', 'tp'), may hold values from -0.125 to 0.125
- gate_in: bfloat16 [2048, 1024], P('sp', 'tp'), may hold values from -0.125 to 0.125
- value_in: bfloat16 [2048, 1024], P('sp', 'tp'), may hold values from -0.125 to 0.125
- pool_mix: bfloat16 [4, 128, 128], P('tp'), may hold values from -0.5 to 0.5
- averaging_factor: float32 [512], P('tp'), may hold values from 0.25 to 0.75
- conv_taps: float32 [4, 1024], P(None, 'tp'), may hold values from -3 to 3
- rate_mix: bfloat16 [16, 64, 64], P('tp'), may hold values from -0.75 to 0.75
- input_mix: bfloat16 [16, 64, 64], P('tp'), may hold values from -0.75 to 0.75
- log_rate: float32 [1024], P('tp'), may hold values from 1.5 to 16
- decay_shift: float32 [32, 4096], P(('fs', 'tp'), 'sp'), parts along dimension 0, may hold values from -1.1 to 0
- initial_state: float32 [2048], P(('fs', 'tp')), parts along dimension 0, may hold values from -6 to 6
- out_pool: bfloat16 [2048, 512], P('sp', 'tp'), may hold values from -0.15625 to 0.15625
- out_rnn: bfloat16 [2048, 1024], P('sp', 'tp'), may hold values from -0.15625 to 0.15625
Outputs:
- mixed: bfloat16 [8192, 2048], P(('fs', 'sp', 'tp')), parts along dimension 0
There are 2 independent parts, one for each index of `fs`. A program takes and returns all parts, laid end to end along the dimension named above; an argument that names none is the same for every part. Nothing has to cross between parts.
All inputs are finite; a program needn't handle non-finite values.
Results may differ from a plain program's by a relative error of at most 0.012.
Values may be sent and summed in bfloat16 or wider, within the bound.
No kernel may reach another device: no remote copies, remote signals or barrier semaphores. Data moves between devices by JAX's collectives and lax.ppermute only.
A program may use at most 64 MiB of HBM per device.

v0:
```python
import jax
import jax.numpy as jnp
from jax import lax
from jax.sharding import PartitionSpec as P

GROUP_WIDTH = 128
HEAD_DIM = 64
TAPS = 4
REACH = 16
epsilon = 1e-06
sharpness = 8.0


def from_behind(value, axis, steps):
    count = lax.axis_size(axis)
    first, last = (max(0, -steps), min(count, count - steps))
    return lax.ppermute(value, axis, [(source, source + steps) for source in range(first, last)])


def carried_in(array, axis, combine, identity):
    count, index = (lax.axis_size(axis), lax.axis_index(axis))
    everything = jax.tree.map(lambda part: lax.all_gather(part, axis), array)
    start = jax.tree.map(
        lambda part, zero: jnp.broadcast_to(jnp.asarray(zero, part.dtype), part.shape),
        array,
        identity,
    )

    def hop(k, before):
        reached = k < index
        new = combine(before, jax.tree.map(lambda part: part[k], everything))
        return jax.tree.map(lambda a, b: jnp.where(reached, a, b), new, before)

    return lax.fori_loop(0, count, hop, start)


def chain_pairs(first_pair, second_pair):
    return (first_pair[0] * second_pair[0], second_pair[0] * first_pair[1] + second_pair[1])


def right_product(left_rows, weight_rows):
    return lax.dot_general(
        left_rows, weight_rows, (((1,), (1,)), ((), ())), preferred_element_type=jnp.float32
    )


def shards(
    tokens,
    norm_gain,
    pool_in,
    gate_in,
    value_in,
    pool_mix,
    averaging_factor,
    conv_taps,
    rate_mix,
    input_mix,
    log_rate,
    decay_shift,
    initial_state,
    out_pool,
    out_rnn,
):
    tp_index = lax.axis_index("tp")
    sp_index = lax.axis_index("sp")
    gathered = (
        lax.all_gather(pool_in, "sp", axis=0, tiled=True),
        lax.all_gather(gate_in, "sp", axis=0, tiled=True),
        lax.all_gather(value_in, "sp", axis=0, tiled=True),
        lax.all_gather(out_pool, "sp", axis=0, tiled=True),
        lax.all_gather(out_rnn, "sp", axis=0, tiled=True),
    )
    pool_weight, gate_weight, value_weight, averaging_exit_matrix, out_rnn_weight = gathered
    pool_width = pool_weight.shape[1]
    rnn_width = gate_weight.shape[1]
    widened = lax.all_gather(tokens, "tp", axis=0, tiled=True).astype(jnp.float32)
    scaling = lax.rsqrt(jnp.mean(widened * widened, axis=1, keepdims=True) + epsilon)
    normed = (widened * scaling * norm_gain[None, :]).astype(jnp.bfloat16)
    outputs = [
        jnp.dot(normed, matrix, preferred_element_type=jnp.float32).astype(jnp.bfloat16)
        for matrix in (pool_weight, gate_weight, value_weight)
    ]
    projected = jnp.concatenate(outputs, axis=1)
    block_rows = projected.shape[0]
    pool_pre = projected[:, :pool_width]
    gate_pre = projected[:, pool_width : pool_width + rnn_width]
    value_pre = projected[:, pool_width + rnn_width :]
    edge_rows = jnp.concatenate(
        [pool_pre[block_rows - REACH :], value_pre[block_rows - REACH :]], axis=1
    )
    earlier_rows = from_behind(edge_rows, "sp", 1)
    pool_values = pool_pre.astype(jnp.float32)
    pool_padded = jnp.concatenate([earlier_rows[:, :pool_width], pool_pre], axis=0).astype(
        jnp.float32
    )
    value_padded = jnp.concatenate([earlier_rows[:, pool_width:], value_pre], axis=0).astype(
        jnp.float32
    )
    groups_here = pool_width // GROUP_WIDTH
    group_index = tp_index * groups_here + jnp.arange(pool_width, dtype=jnp.int32) // GROUP_WIDTH
    window = jnp.left_shift(jnp.int32(2), group_index)
    positions = sp_index * block_rows + jnp.arange(block_rows, dtype=jnp.int32)
    window_sum = jnp.zeros((block_rows, pool_width), jnp.float32)
    for steps_back in range(REACH):
        lagged = pool_padded[REACH - steps_back : REACH - steps_back + block_rows]
        window_sum = window_sum + jnp.where(steps_back < window[None, :], lagged, 0.0)
    counts = jnp.minimum(positions[:, None] + 1, window[None, :]).astype(jnp.float32)
    pooled = (window_sum / counts - pool_values).astype(jnp.bfloat16)
    grouped = pooled.reshape(block_rows, groups_here, GROUP_WIDTH)
    mixed_groups = jnp.einsum("tgc,gcd->tgd", grouped, pool_mix, preferred_element_type=jnp.float32)
    pool_out = (mixed_groups.reshape(block_rows, pool_width) * averaging_factor[None, :]).astype(
        jnp.bfloat16
    )
    start_row = REACH - TAPS + 1
    convolved = conv_taps[0][None, :] * value_padded[start_row : start_row + block_rows]
    for tap_index in range(1, TAPS):
        convolved = (
            convolved
            + conv_taps[tap_index][None, :]
            * value_padded[start_row + tap_index : start_row + tap_index + block_rows]
        )
    conv_out = convolved.astype(jnp.bfloat16)
    heads_here = rnn_width // HEAD_DIM
    both_mixes = jnp.concatenate([rate_mix, input_mix], axis=2)
    gate_terms = jnp.einsum(
        "thc,hcd->thd",
        conv_out.reshape(block_rows, heads_here, HEAD_DIM),
        both_mixes,
        preferred_element_type=jnp.float32,
    )
    rate_gate = jax.nn.sigmoid(gate_terms[:, :, :HEAD_DIM]).reshape(block_rows, rnn_width)
    input_gate = jax.nn.sigmoid(gate_terms[:, :, HEAD_DIM:]).reshape(block_rows, rnn_width)
    shifts = jnp.broadcast_to(
        jnp.transpose(decay_shift)[:, :, None], (block_rows, heads_here, HEAD_DIM)
    ).reshape(block_rows, rnn_width)
    log_decay = -sharpness * rate_gate * jax.nn.softplus(-log_rate)[None, :] + shifts
    decays = jnp.exp(log_decay)
    drives = jnp.sqrt(-jnp.expm1(2.0 * log_decay)) * input_gate * conv_out.astype(jnp.float32)
    cumulative, local_state = lax.associative_scan(chain_pairs, (decays, drives), axis=0)
    identity = (jnp.ones((rnn_width,), jnp.float32), jnp.zeros((rnn_width,), jnp.float32))
    prior_decay, prior_state = carried_in(
        (cumulative[block_rows - 1], local_state[block_rows - 1]), "sp", chain_pairs, identity
    )
    carried = prior_decay * initial_state + prior_state
    hidden_state = local_state + cumulative * carried[None, :]
    rnn_out = (jax.nn.gelu(gate_pre.astype(jnp.float32), approximate=True) * hidden_state).astype(
        jnp.bfloat16
    )
    return lax.psum_scatter(
        right_product(pool_out, averaging_exit_matrix) + right_product(rnn_out, out_rnn_weight),
        "tp",
        scatter_dimension=0,
        tiled=True,
    ).astype(jnp.bfloat16)


def solution(mesh):
    placed = (
        P(("fs", "sp", "tp"), None),
        P(),
        P("sp", "tp"),
        P("sp", "tp"),
        P("sp", "tp"),
        P("tp", None, None),
        P("tp"),
        P(None, "tp"),
        P("tp", None, None),
        P("tp", None, None),
        P("tp"),
        P(("fs", "tp"), "sp"),
        P(("fs", "tp")),
        P("sp", "tp"),
        P("sp", "tp"),
    )
    return jax.shard_map(
        shards, mesh=mesh, in_specs=placed, out_specs=P(("fs", "sp", "tp"), None), check_vma=False
    )
```

profile of v0, /device:TPU:0, one launch (start us, length us, event | category | flops | bytes accessed | tf_op | source)
XLA Modules:
  0.0 381.2 jit_solution(15395088567445469416)
XLA Ops:
  15.7 6.6 %all-gather.9.cloned.1.call-done = bf16[512,2048]{1,0:T(8,128)(2,1)} async-done(((bf16[256,2048]{1,0:T(8,128)(2,1)}), bf16[512,2048]{1,0:T(8,128)(2,1)}) %all-gather.9.cloned.1.call-update) | async-done | bytes 2097168 | tf_op jit(solution)/shard_map/all_gather | solution.py:76
  22.2 2.2 fusion
  24.5 41.4 %all-gather.11.cloned.1.call-done = bf16[2048,256]{1,0:T(8,128)(2,1)} async-done(((bf16[256,256]{1,0:T(8,128)(2,1)}), bf16[2048,256]{1,0:T(8,128)(2,1)}) %all-gather.11.cloned.1.call-update) | async-done | bytes 1048592 | tf_op jit(solution)/shard_map/all_gather | solution.py:67
  68.6 47.2 %all-gather.13.cloned.1.call-done = bf16[2048,512]{1,0:T(8,128)(2,1)} async-done(((bf16[256,512]{1,0:T(8,128)(2,1)}), bf16[2048,512]{1,0:T(8,128)(2,1)}) %all-gather.13.cloned.1.call-update) | async-done | bytes 2097168 | tf_op jit(solution)/shard_map/all_gather | solution.py:69
  115.8 2.9 convolution_convert_fusion.1
  119.5 2.6 collective-permute-start
  132.8 2.5 copy.31
  135.3 2.6 copy.33
  137.9 4.4 %convert_multiply_fusion.5 = (f32[512,512]{1,0:T(8,128)}, f32[512,512]{1,0:T(8,128)}) fusion(f32[512,512]{1,0:T(8,128)} %copy.33, f32[512,512]{1,0:T(8,128)} %copy.32, f32[512,512]{1,0:T(8,128)} %copy.31, f32[512]{0:T(512)S(1)} %fusion.63, f32[528,512]{1,0:T(8,128)S(1)} %maximum_convert_fusion, f32[512]{0:T(512)S(1)} %bitcast.61, f32[512]{0:T(512)S(1)} %bitcast.63, ...), kind=kLoop, calls=%fused_computation.41 | loop fusion | flops 3932160 | bytes 9447424 | tf_op jit(solution)/shard_map/mul | solution.py:138
  142.2 3.7 slice.389
  146.0 3.6 slice.390
  153.7 2.7 multiply_add_fusion.1
  156.5 2.5 slice.395
  158.9 2.5 slice.396
  161.4 2.5 slice.394
  163.9 2.5 slice.398
  229.7 2.5 slice.393
  232.3 2.5 slice.450
  239.5 3.7 slice.452
  253.7 4.6 %pad.127 = f32[512,512]{1,0:T(8,128)} pad(f32[256,512]{1,0:T(8,128)} %add.492, f32[]{:T(128)} %constant.117.clone.1), padding=1_0_1x0_0_0 | pad | bytes 1572868 | tf_op jit(solution)/shard_map/pad | solution.py:139
  260.0 2.6 pad.142
  266.3 2.7 fusion.20
  269.9 4.6 %pad.126 = f32[512,512]{1,0:T(8,128)} pad(f32[256,512]{1,0:T(8,128)} %pad_maximum_fusion, f32[]{:T(128)} %constant.117.clone.1), padding=0_1_1x0_0_0 | pad | bytes 1572868 | tf_op jit(solution)/shard_map/pad | solution.py:139
  275.2 26.7 %all-gather.1 = f32[8,1,512]{2,1,0:T(1,128)S(1)} all-gather(f32[1,1,512]{2,1,0:T(1,128)S(1)} %add_bitcast_fusion), channel_id=1, replica_groups=mesh['sp'=8,'fs'=2,'tp'=2] {'sp'}, dimensions={0}, use_global_device_ids=true | all-gather | bytes 18432 | tf_op jit(solution)/shard_map/all_gather | solution.py:22
  301.9 4.7 %pad.145 = f32[512,512]{1,0:T(8,128)} pad(f32[256,512]{1,0:T(8,128)} %add.502, f32[]{:T(128)} %constant.117.clone.1), padding=1_0_1x0_0_0 | pad | bytes 1572868 | tf_op jit(solution)/shard_map/pad | solution.py:139
  308.6 4.6 %pad.144 = f32[512,512]{1,0:T(8,128)} pad(f32[256,512]{1,0:T(8,128)} %pad_maximum_fusion.1, f32[]{:T(128)} %constant.117.clone.1), padding=0_1_1x0_0_0 | pad | bytes 1572868 | tf_op jit(solution)/shard_map/pad | solution.py:139
  313.9 26.3 %all-gather = f32[8,1,512]{2,1,0:T(1,128)S(1)} all-gather(f32[1,1,512]{2,1,0:T(1,128)S(1)} %add_bitcast_fusion.1), channel_id=1, replica_groups=mesh['sp'=8,'fs'=2,'tp'=2] {'sp'}, dimensions={0}, use_global_device_ids=true | all-gather | bytes 18432 | tf_op jit(solution)/shard_map/all_gather | solution.py:22
  341.6 7.2 %fusion.46 = f32[2,512,128]{1,2,0:T(8,128)S(1)} fusion(bf16[2,128,128]{2,1,0:T(8,128)(2,1)S(1)} %copy-done, bf16[512,256]{1,0:T(8,128)(2,1)S(1)} %copy-done.8, s32[256]{0:T(256)S(1)} %copy-done.46, s32[512]{0:T(512)S(1)} %copy-done.42, f32[528,256]{1,0:T(8,128)} %maximum_convert_fusion.1, pred[256]{0:T(512)(128)(4,1)S(1)} %copy-done.47, ...), kind=kOutput, calls=%fused_computation.93 | convolution fusion | flops 38404096 | bytes 9250560 | tf_op jit(solution)/shard_map/tgc,gcd->tgd/dot_general | solution.py:110
  349.0 4.0 %fusion.77 = f32[512,2048]{1,0:T(8,128)} fusion(bf16[512,256]{0,1:T(8,128)(2,1)S(1)} %fusion.38, bf16[2048,256]{1,0:T(8,128)(2,1)} %all-gather.15.cloned.1.call-done), kind=kOutput, calls=%fused_computation.191 | convolution fusion | flops 536870912 | bytes 5505024 | tf_op jit(solution)/shard_map/dot_general | solution.py:42
  353.0 9.1 %convolution_add_fusion = f32[512,2048]{1,0:T(8,128)} fusion(f32[512,2048]{1,0:T(8,128)} %fusion.77, bf16[2048,512]{1,0:T(8,128)(2,1)} %all-gather.19.cloned.1.call-done, bf16[2048,512]{1,0:T(8,128)(2,1)} %all-gather.17.cloned.1.call-done, f32[512,512]{1,0:T(8,128)} %pad.144, f32[512,512]{1,0:T(8,128)} %pad.145, f32[512,512]{1,0:T(8,128)} %pad.126, ...), kind=kOutput, calls=%fused_computation.9 | convolution fusion | flops 2156920832 | bytes 18886656 | tf_op jit(solution)/shard_map/dot_general | solution.py:42
  362.2 9.4 %reduce-scatter.2.cloned.1.call-done = f32[256,2048]{1,0:T(8,128)} async-done(((f32[512,2048]{1,0:T(8,128)}), f32[256,2048]{1,0:T(8,128)}) %reduce-scatter.2.cloned.1.call-update) | async-done | bytes 2097168 | tf_op jit(solution)/shard_map/reduce_scatter | solution.py:149
  371.6 2.7 convert_element_type.63
  (298 shorter events, 116.5 us)
Async XLA Ops:
  6.5 335.0 %copy-start = (bf16[2,128,128]{2,1,0:T(8,128)(2,1)S(1)}, bf16[2,128,128]{2,1,0:T(8,128)(2,1)}, u32[]{:S(2)}) copy-start(bf16[2,128,128]{2,1,0:T(8,128)(2,1)} %param.22) | copy-start | bytes 196612
  6.5 59.3 %copy-start.23 = (f32[2048]{0:T(1024)S(1)}, f32[2048]{0:T(1024)}, u32[]{:S(2)}) copy-start(f32[2048]{0:T(1024)} %param.18) | copy-start | bytes 24580
  6.5 15.7 %all-gather.9.cloned.1.call-start = ((), (), s32[]{:S(2)}) async-start(), calls=%async_computation.1 | async-start | bytes 3145728 | tf_op jit(solution)/shard_map/all_gather | solution.py:76
  7.3 58.6 %all-gather.11.cloned.1.call-start = ((), (), s32[]{:S(2)}) async-start(), calls=%async_computation.2 | async-start | bytes 1179648 | tf_op jit(solution)/shard_map/all_gather | solution.py:67
  8.0 107.8 %all-gather.13.cloned.1.call-start = ((), (), s32[]{:S(2)}) async-start(), calls=%async_computation.3 | async-start | bytes 2359296 | tf_op jit(solution)/shard_map/all_gather | solution.py:69
  8.8 340.3 %all-gather.15.cloned.1.call-start = ((), (), s32[]{:S(2)}) async-start(), calls=%async_computation.4 | async-start | bytes 1179648 | tf_op jit(solution)/shard_map/all_gather | solution.py:70
  9.3 343.7 %all-gather.17.cloned.1.call-start = ((), (), s32[]{:S(2)}) async-start(), calls=%async_computation.5 | async-start | bytes 2359296 | tf_op jit(solution)/shard_map/all_gather | solution.py:68
  9.9 343.1 %all-gather.19.cloned.1.call-start = ((), (), s32[]{:S(2)}) async-start(), calls=%async_computation.6 | async-start | bytes 2359296 | tf_op jit(solution)/shard_map/all_gather | solution.py:71
  10.5 361.1 %reduce-scatter.2.cloned.1.call-start = ((), (), s32[]{:S(2)}) async-start(), calls=%async_computation.7 | async-start | bytes 6291456 | tf_op jit(solution)/shard_map/reduce_scatter | solution.py:149
  22.2 43.6 %copy-start.1 = (bf16[512,2048]{1,0:T(8,128)(2,1)S(1)}, bf16[512,2048]{1,0:T(8,128)(2,1)}, u32[]{:S(2)}) copy-start(bf16[512,2048]{1,0:T(8,128)(2,1)} %all-gather.9.cloned.1.call-done) | copy-start | bytes 6291460
  24.5 91.3 %copy-start.25 = (f32[512]{0:T(512)}, f32[512]{0:T(512)S(1)}, u32[]{:S(2)}) copy-start(f32[512]{0:T(512)S(1)} %add_rsqrt_fusion) | copy-start | bytes 6148
  68.6 54.1 %copy-start.20 = (f32[8,512]{1,0:T(8,128)S(1)}, f32[8,512]{1,0:T(8,128)}, u32[]{:S(2)}) copy-start(f32[8,512]{1,0:T(8,128)} %param.28) | copy-start | bytes 49156
  119.5 4.6 %collective-permute-start = (bf16[16,768]{1,0:T(8,128)(2,1)S(1)}, bf16[16,768]{1,0:T(8,128)(2,1)S(1)}, u32[]{:S(2)}, u32[]{:S(2)}) collective-permute-start(bf16[16,768]{1,0:T(8,128)(2,1)S(1)} %pad_maximum_fusion.10), channel_id=1, source_target_pairs={{0,4},{4,8},{8,12},{12,16},{16,20},{20,24},{24,28},{1,5},{5,9},{9,... | collective-permute-start | bytes 73736 | tf_op jit(solution)/shard_map/ppermute | solution.py:17
  229.7 15.7 %copy-start.35 = (f32[1,512]{1,0:T(1,128)S(1)}, f32[1,512]{1,0:T(1,128)}, u32[]{:S(2)}) copy-start(f32[1,512]{1,0:T(1,128)} %slice.504) | copy-start | bytes 6148
  229.7 15.7 %copy-start.16 = (f32[7,512]{1,0:T(8,128)S(1)}, f32[7,512]{1,0:T(8,128)}, u32[]{:S(2)}) copy-start(f32[7,512]{1,0:T(8,128)} %slice.442) | copy-start | bytes 43012
  229.7 15.8 %copy-start.34 = (f32[1,512]{1,0:T(1,128)S(1)}, f32[1,512]{1,0:T(1,128)}, u32[]{:S(2)}) copy-start(f32[1,512]{1,0:T(1,128)} %slice.532) | copy-start | bytes 6148
  229.7 15.8 %copy-start.33 = (f32[1,512]{1,0:T(1,128)S(1)}, f32[1,512]{1,0:T(1,128)}, u32[]{:S(2)}) copy-start(f32[1,512]{1,0:T(1,128)} %slice.503) | copy-start | bytes 6148
  229.7 15.9 %copy-start.12 = (f32[15,512]{1,0:T(8,128)S(1)}, f32[15,512]{1,0:T(8,128)}, u32[]{:S(2)}) copy-start(f32[15,512]{1,0:T(8,128)} %slice.411) | copy-start | bytes 92164
  229.7 15.9 %copy-start.13 = (f32[15,512]{1,0:T(8,128)S(1)}, f32[15,512]{1,0:T(8,128)}, u32[]{:S(2)}) copy-start(f32[15,512]{1,0:T(8,128)} %slice.444) | copy-start | bytes 92164
  269.0 37.6 %copy-start.27 = (f32[1,512]{1,0:T(1,128)S(1)}, f32[1,512]{1,0:T(1,128)}, u32[]{:S(2)}) copy-start(f32[1,512]{1,0:T(1,128)} %slice.527) | copy-start | bytes 6148
  301.9 38.4 %copy-start.8 = (bf16[512,256]{1,0:T(8,128)(2,1)S(1)}, bf16[512,256]{1,0:T(8,128)(2,1)}, u32[]{:S(2)}) copy-start(bf16[512,256]{1,0:T(8,128)(2,1)} %copy-done.7) | copy-start | bytes 786436
  301.9 38.4 %slice-start = ((bf16[16,768]{1,0:T(8,128)(2,1)}), bf16[16,256]{1,0:T(8,128)(2,1)S(1)}, s32[]{:S(2)}) async-start(bf16[16,768]{1,0:T(8,128)(2,1)} %copy-done.17), calls=%async_computation.8 | async-start | bytes 16384 | tf_op jit(solution)/shard_map/slice | solution.py:93
  306.6 34.5 %copy-start.14 = (f32[512]{0:T(512)S(1)}, f32[512]{0:T(512)}, u32[]{:S(2)}) copy-start(f32[512]{0:T(512)} %custom-call) | copy-start | bytes 6148
  306.6 34.5 %copy-start.15 = (f32[512]{0:T(512)S(1)}, f32[512]{0:T(512)}, u32[]{:S(2)}) copy-start(f32[512]{0:T(512)} %custom-call.1) | copy-start | bytes 6148
  306.6 34.9 %copy-start.44 = (f32[512]{0:T(512)S(1)}, f32[512]{0:T(512)}, u32[]{:S(2)}) copy-start(f32[512]{0:T(512)} %param.29) | copy-start | bytes 6148
  306.6 35.0 %copy-start.42 = (s32[512]{0:T(512)S(1)}, s32[512]{0:T(512)}, u32[]{:S(2)}) copy-start(s32[512]{0:T(512)} %add_add_fusion) | copy-start | bytes 6148
  306.6 35.0 %copy-start.46 = (s32[256]{0:T(256)S(1)}, s32[256]{0:T(256)}, u32[]{:S(2)}) copy-start(s32[256]{0:T(256)} %fusion.65) | copy-start | bytes 3076
  306.6 35.0 %copy-start.47 = (pred[256]{0:T(512)(128)(4,1)S(1)}, pred[256]{0:T(512)(128)(4,1)}, u32[]{:S(2)}) copy-start(pred[256]{0:T(512)(128)(4,1)} %get-tuple-element.200) | copy-start | bytes 772
  306.6 35.0 %copy-start.48 = (pred[256]{0:T(512)(128)(4,1)S(1)}, pred[256]{0:T(512)(128)(4,1)}, u32[]{:S(2)}) copy-start(pred[256]{0:T(512)(128)(4,1)} %get-tuple-element.201) | copy-start | bytes 772
  306.6 35.0 %copy-start.49 = (pred[256]{0:T(512)(128)(4,1)S(1)}, pred[256]{0:T(512)(128)(4,1)}, u32[]{:S(2)}) copy-start(pred[256]{0:T(512)(128)(4,1)} %get-tuple-element.202) | copy-start | bytes 772
  306.6 35.0 %copy-start.50 = (pred[256]{0:T(512)(128)(4,1)S(1)}, pred[256]{0:T(512)(128)(4,1)}, u32[]{:S(2)}) copy-start(pred[256]{0:T(512)(128)(4,1)} %get-tuple-element.203) | copy-start | bytes 772
  306.6 35.0 %copy-start.51 = (pred[256]{0:T(512)(128)(4,1)S(1)}, pred[256]{0:T(512)(128)(4,1)}, u32[]{:S(2)}) copy-start(pred[256]{0:T(512)(128)(4,1)} %get-tuple-element.204) | copy-start | bytes 772
  (29 other events, 225.5 us)
Sparse Core Ops, SparseCore 0:
  8.9 13.2 all-gather.8
  24.3 41.4 all-gather.10
  68.0 47.7 all-gather.12
  117.8 38.7 all-gather.14
  158.6 47.7 all-gather.16
  208.4 47.6 all-gather.18
  362.3 9.2 reduce-scatter.1
where the time goes:
time: 385 us; the launch traced here: 381 us
  local copies, waits for them, and re-layouts  123 us (32%)
  waiting for transfers between devices  108 us (28%)
  blocking collectives  53 us (14%)
  other arithmetic  52.5 us (14%)
  matrix products  26.8 us (7%)
  between operations  14.5 us (4%)
    slice x60, local copies, waits for them, and re-layouts, shards(): lax.associative_scan(chain_pairs, (decays, drives), axis=0)  87.8 us
    all_gather x2, blocking collectives, carried_in(): everything = jax.tree.map(lambda part: lax.all_gather(part, axis), array)  53 us
    all_gather x1, waiting for transfers between devices, shards(): lax.all_gather(value_in, 'sp', axis=0, tiled=True)  47.2 us
    all_gather x1, waiting for transfers between devices, shards(): lax.all_gather(pool_in, 'sp', axis=0, tiled=True)  41.4 us
    pad x32, local copies, waits for them, and re-layouts, shards(): lax.associative_scan(chain_pairs, (decays, drives), axis=0)  24.2 us
    add x16, other arithmetic, chain_pairs(): second_pair[0] * first_pair[1] + second_pair[1]  17.6 us
    dot_general x2, matrix products, right_product(): lax.dot_general(left_rows, weight_rows, (((1,), (1,)), ((), ())), preferr...  13.1 us
    reduce_scatter x1, waiting for transfers between devices, shards(): lax.psum_scatter(right_product(pool_out, averaging_exit_matrix) + right_p...  9.43 us
  transfers between devices with their start and end apart: 8, of which 4 were waited for; matrix products, arithmetic and copies ran while one was open for 49% of the time, Pallas kernels for 0%

commit v1 on v0

--- a/solution.py
+++ b/solution.py
@@ -1,3 +1,4 @@
+import functools
 import jax
 import jax.numpy as jnp
 from jax import lax
@@ -9,6 +10,16 @@
 REACH = 16
 epsilon = 1e-06
 sharpness = 8.0
+
+
+def link_state(local_values, array_axis):
+    a_now = jnp.stack([local_values for _ in range(lax.axis_size("sp"))])
+    side_arr = lax.all_to_all(a_now, "sp", 0, 0)
+    back = jnp.concatenate(side_arr, array_axis)
+    return back
+
+
+_update_sizes = functools.partial(link_state, array_axis=0)
 
 
 def from_behind(value, axis, steps):
@@ -66,7 +77,7 @@
     gathered = (
         lax.all_gather(pool_in, "sp", axis=0, tiled=True),
         lax.all_gather(gate_in, "sp", axis=0, tiled=True),
-        lax.all_gather(value_in, "sp", axis=0, tiled=True),
+        _update_sizes(value_in),
         lax.all_gather(out_pool, "sp", axis=0, tiled=True),
         lax.all_gather(out_rnn, "sp", axis=0, tiled=True),
     )

time: 385 us -> 354 us (0.919)
  waiting for transfers between devices: 108 us -> 66.2 us
  starting transfers between devices: 2.89 us -> 11 us
    all_gather x1 -> x0, waiting for transfers between devices: 47.2 us -> none  [shards(): lax.all_gather(value_in, 'sp', axis=0, tiled=True)]
    all_gather x1, waiting for transfers between devices: 41.4 us -> 53.6 us  [shards(): lax.all_gather(pool_in, 'sp', axis=0, tiled=True)]
    all_to_all x0 -> x1, starting transfers between devices: none -> 7.44 us  [link_state(): side_arr = lax.all_to_all(a_now, 'sp', 0, 0)]
    all_gather x1, waiting for transfers between devices: 6.56 us -> 0.02 us  [shards(): lax.all_gather(tokens, 'tp', axis=0, tiled=True).astype(jnp.float32)]
  transfers between devices with their start and end apart: 8 -> 8, of which waited for: 4 -> 2; matrix products, arithmetic and copies ran while one was open for 49% -> 55% of each run, Pallas kernels for 0% -> 0%
where the time goes in v1:
time: 354 us; the launch traced here: 350 us
  local copies, waits for them, and re-layouts  126 us (36%)
  waiting for transfers between devices  66.2 us (19%)
  blocking collectives  53.2 us (15%)
  other arithmetic  53 us (15%)
  matrix products  26.5 us (7%)
  between operations  14.5 us (4%)
  starting transfers between devices  11 us (3%)
    slice x60, local copies, waits for them, and re-layouts, shards(): lax.associative_scan(chain_pairs, (decays, drives), axis=0)  88 us
    all_gather x1, waiting for transfers between devices, shards(): lax.all_gather(pool_in, 'sp', axis=0, tiled=True)  53.6 us
    all_gather x2, blocking collectives, carried_in(): everything = jax.tree.map(lambda part: lax.all_gather(part, axis), array)  53.2 us
    pad x32, local copies, waits for them, and re-layouts, shards(): lax.associative_scan(chain_pairs, (decays, drives), axis=0)  24.3 us
    add x16, other arithmetic, chain_pairs(): second_pair[0] * first_pair[1] + second_pair[1]  17.8 us
    dot_general x2, matrix products, right_product(): lax.dot_general(left_rows, weight_rows, (((1,), (1,)), ((), ())), preferr...  13.1 us
    reduce_scatter x1, waiting for transfers between devices, shards(): lax.psum_scatter(right_product(pool_out, averaging_exit_matrix) + right_p...  9.4 us
    all_to_all x1, starting transfers between devices, link_state(): side_arr = lax.all_to_all(a_now, 'sp', 0, 0)  7.44 us
  transfers between devices with their start and end apart: 8, of which 2 were waited for; matrix products, arithmetic and copies ran while one was open for 55% of the time, Pallas kernels for 0%

profile of v1, /device:TPU:0, one launch (start us, length us, event | category | flops | bytes accessed | tf_op | source)
XLA Modules:
  0.0 350.3 jit_solution(1891000158695628767)
XLA Ops:
  9.3 2.4 stack.2
  11.8 7.4 %all-to-all-start = ((bf16[8,256,512]{2,1,0:T(8,128)(2,1)}), bf16[8,256,512]{2,1,0:T(8,128)(2,1)}, u32[]{:S(2)}, u32[]{:S(2)}) async-start(bf16[8,256,512]{2,1,0:T(8,128)(2,1)} %stack.2), calls=%async_computation | async-start | bytes 4194304 | tf_op jit(solution)/shard_map/all_to_all | solution.py:17
  25.2 2.2 fusion
  27.5 53.6 %all-gather.10.cloned.1.call-done = bf16[2048,256]{1,0:T(8,128)(2,1)} async-done(((bf16[256,256]{1,0:T(8,128)(2,1)}), bf16[2048,256]{1,0:T(8,128)(2,1)}) %all-gather.10.cloned.1.call-update) | async-done | bytes 1048592 | tf_op jit(solution)/shard_map/all_gather | solution.py:78
  83.7 2.9 convolution_convert_fusion.1
  87.4 3.4 collective-permute-start
  101.4 2.5 copy.31
  104.0 2.5 copy.33
  106.5 4.5 %convert_multiply_fusion.5 = (f32[512,512]{1,0:T(8,128)}, f32[512,512]{1,0:T(8,128)}) fusion(f32[512,512]{1,0:T(8,128)} %copy.33, f32[512,512]{1,0:T(8,128)} %copy.32, f32[512,512]{1,0:T(8,128)} %copy.31, f32[512]{0:T(512)S(1)} %fusion.63, f32[528,512]{1,0:T(8,128)S(1)} %maximum_convert_fusion, f32[512]{0:T(512)S(1)} %bitcast.62, f32[512]{0:T(512)S(1)} %bitcast.64, ...), kind=kLoop, calls=%fused_computation.41 | loop fusion | flops 3932160 | bytes 9447424 | tf_op jit(solution)/shard_map/mul | solution.py:149
  111.0 3.8 %slice.389 = f32[256,512]{1,0:T(8,128)} slice(f32[512,512]{1,0:T(8,128)} %get-tuple-element.154), slice={[0:511:2], [0:512:1]} | slice | bytes 1048576 | tf_op jit(solution)/shard_map/slice | solution.py:150
  114.8 3.6 %slice.390 = f32[256,512]{1,0:T(8,128)} slice(f32[512,512]{1,0:T(8,128)} %get-tuple-element.154), slice={[1:512:2], [0:512:1]} | slice | bytes 1048576 | tf_op jit(solution)/shard_map/slice | solution.py:150
  122.6 2.7 multiply_add_fusion.1
  125.3 2.5 slice.395
  127.8 2.5 slice.396
  130.3 2.5 slice.394
  132.8 2.5 slice.398
  199.0 2.5 slice.393
  201.5 2.5 slice.450
  208.7 3.7 %slice.452 = f32[255,512]{1,0:T(8,128)} slice(f32[512,512]{1,0:T(8,128)} %get-tuple-element.154), slice={[2:512:2], [0:512:1]} | slice | bytes 1044480 | tf_op jit(solution)/shard_map/slice | solution.py:150
  223.0 4.6 %pad.127 = f32[512,512]{1,0:T(8,128)} pad(f32[256,512]{1,0:T(8,128)} %add.492, f32[]{:T(128)} %constant.117.clone.1), padding=1_0_1x0_0_0 | pad | bytes 1572868 | tf_op jit(solution)/shard_map/pad | solution.py:150
  229.3 2.7 pad.142
  235.7 2.7 fusion.20
  239.2 4.6 %pad.126 = f32[512,512]{1,0:T(8,128)} pad(f32[256,512]{1,0:T(8,128)} %pad_maximum_fusion, f32[]{:T(128)} %constant.117.clone.1), padding=0_1_1x0_0_0 | pad | bytes 1572868 | tf_op jit(solution)/shard_map/pad | solution.py:150
  244.6 26.8 %all-gather.1 = f32[8,1,512]{2,1,0:T(1,128)S(1)} all-gather(f32[1,1,512]{2,1,0:T(1,128)S(1)} %add_bitcast_fusion), channel_id=1, replica_groups=mesh['sp'=8,'fs'=2,'tp'=2] {'sp'}, dimensions={0}, use_global_device_ids=true | all-gather | bytes 18432 | tf_op jit(solution)/shard_map/all_gather | solution.py:33
  271.4 4.6 %pad.145 = f32[512,512]{1,0:T(8,128)} pad(f32[256,512]{1,0:T(8,128)} %add.502, f32[]{:T(128)} %constant.117.clone.1), padding=1_0_1x0_0_0 | pad | bytes 1572868 | tf_op jit(solution)/shard_map/pad | solution.py:150
  278.0 4.6 %pad.144 = f32[512,512]{1,0:T(8,128)} pad(f32[256,512]{1,0:T(8,128)} %pad_maximum_fusion.1, f32[]{:T(128)} %constant.117.clone.1), padding=0_1_1x0_0_0 | pad | bytes 1572868 | tf_op jit(solution)/shard_map/pad | solution.py:150
  283.3 26.3 %all-gather = f32[8,1,512]{2,1,0:T(1,128)S(1)} all-gather(f32[1,1,512]{2,1,0:T(1,128)S(1)} %add_bitcast_fusion.1), channel_id=1, replica_groups=mesh['sp'=8,'fs'=2,'tp'=2] {'sp'}, dimensions={0}, use_global_device_ids=true | all-gather | bytes 18432 | tf_op jit(solution)/shard_map/all_gather | solution.py:33
  311.1 6.9 %fusion.46 = f32[2,512,128]{1,2,0:T(8,128)S(1)} fusion(bf16[2,128,128]{2,1,0:T(8,128)(2,1)S(1)} %copy-done, bf16[512,256]{1,0:T(8,128)(2,1)S(1)} %copy-done.8, s32[256]{0:T(256)S(1)} %copy-done.46, s32[512]{0:T(512)S(1)} %copy-done.42, f32[528,256]{1,0:T(8,128)} %maximum_convert_fusion.1, pred[256]{0:T(512)(128)(4,1)S(1)} %copy-done.47, ...), kind=kOutput, calls=%fused_computation.93 | convolution fusion | flops 38404096 | bytes 9250560 | tf_op jit(solution)/shard_map/tgc,gcd->tgd/dot_general | solution.py:121
  318.2 4.0 %fusion.77 = f32[512,2048]{1,0:T(8,128)} fusion(bf16[512,256]{0,1:T(8,128)(2,1)S(1)} %fusion.38, bf16[2048,256]{1,0:T(8,128)(2,1)} %all-gather.12.cloned.1.call-done), kind=kOutput, calls=%fused_computation.191 | convolution fusion | flops 536870912 | bytes 5505024 | tf_op jit(solution)/shard_map/dot_general | solution.py:53
  322.2 9.1 %convolution_add_fusion = f32[512,2048]{1,0:T(8,128)} fusion(f32[512,2048]{1,0:T(8,128)} %fusion.77, bf16[2048,512]{1,0:T(8,128)(2,1)} %all-gather.16.cloned.1.call-done, bf16[2048,512]{1,0:T(8,128)(2,1)} %all-gather.14.cloned.1.call-done, f32[512,512]{1,0:T(8,128)} %pad.144, f32[512,512]{1,0:T(8,128)} %pad.145, f32[512,512]{1,0:T(8,128)} %pad.126, ...), kind=kOutput, calls=%fused_computation.9 | convolution fusion | flops 2156920832 | bytes 18886656 | tf_op jit(solution)/shard_map/dot_general | solution.py:53
  331.3 9.4 %reduce-scatter.2.cloned.1.call-done = f32[256,2048]{1,0:T(8,128)} async-done(((f32[512,2048]{1,0:T(8,128)}), f32[256,2048]{1,0:T(8,128)}) %reduce-scatter.2.cloned.1.call-update) | async-done | bytes 2097168 | tf_op jit(solution)/shard_map/reduce_scatter | solution.py:160
  340.7 2.7 convert_element_type.63
  (298 shorter events, 116.5 us)
Async XLA Ops:
  6.5 304.4 %copy-start = (bf16[2,128,128]{2,1,0:T(8,128)(2,1)S(1)}, bf16[2,128,128]{2,1,0:T(8,128)(2,1)}, u32[]{:S(2)}) copy-start(bf16[2,128,128]{2,1,0:T(8,128)(2,1)} %param.22) | copy-start | bytes 196612
  6.5 18.7 %all-gather.8.cloned.1.call-start = ((), (), s32[]{:S(2)}) async-start(), calls=%async_computation.2 | async-start | bytes 3145728 | tf_op jit(solution)/shard_map/all_gather | solution.py:87
  7.3 73.8 %all-gather.10.cloned.1.call-start = ((), (), s32[]{:S(2)}) async-start(), calls=%async_computation.3 | async-start | bytes 1179648 | tf_op jit(solution)/shard_map/all_gather | solution.py:78
  8.0 310.2 %all-gather.12.cloned.1.call-start = ((), (), s32[]{:S(2)}) async-start(), calls=%async_computation.4 | async-start | bytes 1179648 | tf_op jit(solution)/shard_map/all_gather | solution.py:81
  8.7 313.4 %all-gather.14.cloned.1.call-start = ((), (), s32[]{:S(2)}) async-start(), calls=%async_computation.5 | async-start | bytes 2359296 | tf_op jit(solution)/shard_map/all_gather | solution.py:79
  11.8 72.0 %all-to-all-start = ((bf16[8,256,512]{2,1,0:T(8,128)(2,1)}), bf16[8,256,512]{2,1,0:T(8,128)(2,1)}, u32[]{:S(2)}, u32[]{:S(2)}) async-start(bf16[8,256,512]{2,1,0:T(8,128)(2,1)} %stack.2), calls=%async_computation | async-start | bytes 4194304 | tf_op jit(solution)/shard_map/all_to_all | solution.py:17
  19.2 61.8 %copy-start.23 = (f32[2048]{0:T(1024)S(1)}, f32[2048]{0:T(1024)}, u32[]{:S(2)}) copy-start(f32[2048]{0:T(1024)} %param.18) | copy-start | bytes 24580
  19.2 303.0 %all-gather.16.cloned.1.call-start = ((), (), s32[]{:S(2)}) async-start(), calls=%async_computation.6 | async-start | bytes 2359296 | tf_op jit(solution)/shard_map/all_gather | solution.py:82
  19.8 320.9 %reduce-scatter.2.cloned.1.call-start = ((), (), s32[]{:S(2)}) async-start(), calls=%async_computation.7 | async-start | bytes 6291456 | tf_op jit(solution)/shard_map/reduce_scatter | solution.py:160
  25.2 55.8 %copy-start.1 = (bf16[512,2048]{1,0:T(8,128)(2,1)S(1)}, bf16[512,2048]{1,0:T(8,128)(2,1)}, u32[]{:S(2)}) copy-start(bf16[512,2048]{1,0:T(8,128)(2,1)} %all-gather.8.cloned.1.call-done) | copy-start | bytes 6291460
  27.5 56.3 %copy-start.25 = (f32[512]{0:T(512)}, f32[512]{0:T(512)S(1)}, u32[]{:S(2)}) copy-start(f32[512]{0:T(512)S(1)} %add_rsqrt_fusion) | copy-start | bytes 6148
  87.4 5.4 %collective-permute-start = (bf16[16,768]{1,0:T(8,128)(2,1)S(1)}, bf16[16,768]{1,0:T(8,128)(2,1)S(1)}, u32[]{:S(2)}, u32[]{:S(2)}) collective-permute-start(bf16[16,768]{1,0:T(8,128)(2,1)S(1)} %pad_maximum_fusion.10), channel_id=1, source_target_pairs={{0,4},{4,8},{8,12},{12,16},{16,20},{20,24},{24,28},{1,5},{5,9},{9,... | collective-permute-start | bytes 73736 | tf_op jit(solution)/shard_map/ppermute | solution.py:28
  198.9 15.5 %copy-start.36 = (f32[1,512]{1,0:T(1,128)S(1)}, f32[1,512]{1,0:T(1,128)}, u32[]{:S(2)}) copy-start(f32[1,512]{1,0:T(1,128)} %slice.533) | copy-start | bytes 6148
  198.9 15.6 %copy-start.35 = (f32[1,512]{1,0:T(1,128)S(1)}, f32[1,512]{1,0:T(1,128)}, u32[]{:S(2)}) copy-start(f32[1,512]{1,0:T(1,128)} %slice.504) | copy-start | bytes 6148
  198.9 15.7 %copy-start.16 = (f32[7,512]{1,0:T(8,128)S(1)}, f32[7,512]{1,0:T(8,128)}, u32[]{:S(2)}) copy-start(f32[7,512]{1,0:T(8,128)} %slice.442) | copy-start | bytes 43012
  198.9 15.7 %copy-start.34 = (f32[1,512]{1,0:T(1,128)S(1)}, f32[1,512]{1,0:T(1,128)}, u32[]{:S(2)}) copy-start(f32[1,512]{1,0:T(1,128)} %slice.532) | copy-start | bytes 6148
  198.9 15.8 %copy-start.33 = (f32[1,512]{1,0:T(1,128)S(1)}, f32[1,512]{1,0:T(1,128)}, u32[]{:S(2)}) copy-start(f32[1,512]{1,0:T(1,128)} %slice.503) | copy-start | bytes 6148
  198.9 15.8 %copy-start.12 = (f32[15,512]{1,0:T(8,128)S(1)}, f32[15,512]{1,0:T(8,128)}, u32[]{:S(2)}) copy-start(f32[15,512]{1,0:T(8,128)} %slice.411) | copy-start | bytes 92164
  198.9 15.8 %copy-start.13 = (f32[15,512]{1,0:T(8,128)S(1)}, f32[15,512]{1,0:T(8,128)}, u32[]{:S(2)}) copy-start(f32[15,512]{1,0:T(8,128)} %slice.444) | copy-start | bytes 92164
  238.4 37.7 %copy-start.27 = (f32[1,512]{1,0:T(1,128)S(1)}, f32[1,512]{1,0:T(1,128)}, u32[]{:S(2)}) copy-start(f32[1,512]{1,0:T(1,128)} %slice.527) | copy-start | bytes 6148
  271.4 38.2 %copy-start.8 = (bf16[512,256]{1,0:T(8,128)(2,1)S(1)}, bf16[512,256]{1,0:T(8,128)(2,1)}, u32[]{:S(2)}) copy-start(bf16[512,256]{1,0:T(8,128)(2,1)} %copy-done.7) | copy-start | bytes 786436
  271.4 38.2 %slice-start = ((bf16[16,768]{1,0:T(8,128)(2,1)}), bf16[16,256]{1,0:T(8,128)(2,1)S(1)}, s32[]{:S(2)}) async-start(bf16[16,768]{1,0:T(8,128)(2,1)} %copy-done.17), calls=%async_computation.8 | async-start | bytes 16384 | tf_op jit(solution)/shard_map/slice | solution.py:104
  276.0 34.5 %copy-start.14 = (f32[512]{0:T(512)S(1)}, f32[512]{0:T(512)}, u32[]{:S(2)}) copy-start(f32[512]{0:T(512)} %custom-call) | copy-start | bytes 6148
  276.0 34.5 %copy-start.15 = (f32[512]{0:T(512)S(1)}, f32[512]{0:T(512)}, u32[]{:S(2)}) copy-start(f32[512]{0:T(512)} %custom-call.1) | copy-start | bytes 6148
  276.0 34.9 %copy-start.44 = (f32[512]{0:T(512)S(1)}, f32[512]{0:T(512)}, u32[]{:S(2)}) copy-start(f32[512]{0:T(512)} %param.29) | copy-start | bytes 6148
  276.0 35.0 %copy-start.42 = (s32[512]{0:T(512)S(1)}, s32[512]{0:T(512)}, u32[]{:S(2)}) copy-start(s32[512]{0:T(512)} %add_add_fusion) | copy-start | bytes 6148
  276.0 35.0 %copy-start.46 = (s32[256]{0:T(256)S(1)}, s32[256]{0:T(256)}, u32[]{:S(2)}) copy-start(s32[256]{0:T(256)} %fusion.65) | copy-start | bytes 3076
  276.0 35.0 %copy-start.47 = (pred[256]{0:T(512)(128)(4,1)S(1)}, pred[256]{0:T(512)(128)(4,1)}, u32[]{:S(2)}) copy-start(pred[256]{0:T(512)(128)(4,1)} %get-tuple-element.200) | copy-start | bytes 772
  276.0 35.0 %copy-start.48 = (pred[256]{0:T(512)(128)(4,1)S(1)}, pred[256]{0:T(512)(128)(4,1)}, u32[]{:S(2)}) copy-start(pred[256]{0:T(512)(128)(4,1)} %get-tuple-element.201) | copy-start | bytes 772
  276.1 35.0 %copy-start.49 = (pred[256]{0:T(512)(128)(4,1)S(1)}, pred[256]{0:T(512)(128)(4,1)}, u32[]{:S(2)}) copy-start(pred[256]{0:T(512)(128)(4,1)} %get-tuple-element.202) | copy-start | bytes 772
  276.1 35.0 %copy-start.50 = (pred[256]{0:T(512)(128)(4,1)S(1)}, pred[256]{0:T(512)(128)(4,1)}, u32[]{:S(2)}) copy-start(pred[256]{0:T(512)(128)(4,1)} %get-tuple-element.203) | copy-start | bytes 772
  276.1 35.0 %copy-start.51 = (pred[256]{0:T(512)(128)(4,1)S(1)}, pred[256]{0:T(512)(128)(4,1)}, u32[]{:S(2)}) copy-start(pred[256]{0:T(512)(128)(4,1)} %get-tuple-element.204) | copy-start | bytes 772
  (29 other events, 226.7 us)
Sparse Core Ops, SparseCore 0:
  8.9 13.2 all-gather.7
  24.3 56.6 all-gather.9
  83.2 39.7 all-gather.11
  124.9 47.7 all-gather.13
  174.7 47.6 all-gather.15
  331.5 9.2 reduce-scatter.1
